TPU v7x, 32 devices: a whole 2x2x4 slice. The times are simulated.
32 devices in a mesh: rep: 2 (over x), fs: 8 (over z, y), tp: 2 (over core).
Axes of the slice: x: 2, y: 2, z: 4, core: 2. Of those that a mesh axis runs over, the one named last changes fastest.
Arguments:
- x_next: bfloat16 [6144, 2048], P(('rep', 'fs')), may hold values from -6 to 6
- value_next: bfloat16 [6144, 3072], P(('rep', 'fs'), 'tp'), may hold values from -6 to 6
- x_prev: bfloat16 [6144, 2048], P(('rep', 'fs')), may hold values from -6 to 6
- value_prev: bfloat16 [6144, 3072], P(('rep', 'fs'), 'tp'), may hold values from -6 to 6
- cotangent: bfloat16 [6144, 3072], P(('rep', 'fs'), 'tp'), may hold values from -6 to 6
- w_gate: bfloat16 [2048, 3072], P('fs', 'tp'), may hold values from -0.125 to 0.125
- conv_taps: float32 [3, 3072], P(None, 'tp'), may hold values from -3.5 to 3.5
- conv_bias: float32 [3072], P('tp'), may hold values from -3 to 3
- sum_w: float32 [2048, 3072], P('fs', 'tp'), may hold values from -6 to 6
- sum_taps: float32 [3, 3072], P(None, 'tp'), may hold values from -6 to 6
- sum_bias: float32 [3072], P('tp'), may hold values from -6 to 6
Outputs:
- hidden_next: bfloat16 [6144, 3072], P(('rep', 'fs'), 'tp')
- grad_input: bfloat16 [6144, 2048], P(('rep', 'fs'))
- grad_value: bfloat16 [6144, 3072], P(('rep', 'fs'), 'tp')
- new_sum_w: float32 [2048, 3072], P('fs', 'tp')
- new_sum_taps: float32 [3, 3072], P(None, 'tp')
- new_sum_bias: float32 [3072], P('tp')
All inputs are finite; a program needn't handle non-finite values.
Results may differ from a plain program's by a relative error of at most 0.015.
Values may be sent and summed in bfloat16 or wider, within the bound.
A program may use at most 64 MiB of HBM per device.

v0:
```python
import jax
import jax.numpy as jnp
from jax import lax
from jax.sharding import PartitionSpec as P

SEQ_LEN = 128


def lagged(values, offset, position):
    count_rows = values.shape[0]
    shifted_rows = jnp.concatenate(
        (jnp.zeros((offset, values.shape[1]), values.dtype), values[: count_rows - offset]), axis=0
    )
    return jnp.where((position >= offset)[:, None], shifted_rows, jnp.zeros_like(shifted_rows))


def leading(values, offset, position):
    shifted_rows = jnp.concatenate(
        (values[offset:], jnp.zeros((offset, values.shape[1]), values.dtype)), axis=0
    )
    return jnp.where(
        (position < SEQ_LEN - offset)[:, None], shifted_rows, jnp.zeros_like(shifted_rows)
    )


def convolve(up_rows, conv_taps, conv_bias, position):
    values = up_rows.astype(jnp.float32)
    tap_count = conv_taps.shape[0]
    result = jnp.zeros(values.shape, jnp.float32) + conv_bias[None, :]
    for tap_index in range(tap_count):
        result = result + conv_taps[tap_index][None, :] * lagged(
            values, tap_count - 1 - tap_index, position
        )
    return result


def per_device(
    x_next,
    value_next,
    x_prev,
    value_prev,
    cotangent,
    w_gate,
    conv_taps,
    conv_bias,
    sum_w,
    sum_taps,
    sum_bias,
):
    row_count = x_next.shape[0]
    tap_count = conv_taps.shape[0]
    position = jnp.arange(row_count) % SEQ_LEN
    gathered = lax.all_gather(w_gate, "fs", axis=0, tiled=True)
    up_next = jnp.dot(x_next, gathered, preferred_element_type=jnp.float32)
    up_prev = jnp.dot(x_prev, gathered, preferred_element_type=jnp.float32)
    up_next = up_next.astype(jnp.bfloat16)
    up_prev = up_prev.astype(jnp.bfloat16)
    gate_next = convolve(up_next, conv_taps, conv_bias, position)
    hidden_next = (gate_next * jax.nn.sigmoid(gate_next) * value_next.astype(jnp.float32)).astype(
        jnp.bfloat16
    )
    gate_prev = convolve(up_prev, conv_taps, conv_bias, position)
    sigmoid_gate = jax.nn.sigmoid(gate_prev)
    cot_values = cotangent.astype(jnp.float32)
    grad_value = (cot_values * gate_prev * sigmoid_gate).astype(jnp.bfloat16)
    grad_gate = (
        cot_values
        * value_prev.astype(jnp.float32)
        * sigmoid_gate
        * (1.0 + gate_prev * (1.0 - sigmoid_gate))
    )
    grad_up = jnp.zeros(grad_gate.shape, jnp.float32)
    for tap_index in range(tap_count):
        grad_up = grad_up + conv_taps[tap_index][None, :] * leading(
            grad_gate, tap_count - 1 - tap_index, position
        )
    grad_up = grad_up.astype(jnp.bfloat16)
    contract_units = (((1,), (1,)), ((), ()))
    partial_input = lax.dot_general(
        grad_up, gathered, contract_units, preferred_element_type=jnp.float32
    )
    grad_input = lax.psum(partial_input.astype(jnp.bfloat16), "tp")
    rep_count = lax.axis_size("rep")
    fs_count = lax.axis_size("fs")
    grad_scale = float(row_count * rep_count * fs_count) ** (-0.5)
    up_values = up_prev.astype(jnp.float32)
    tap_terms = (
        jnp.stack(
            [
                jnp.sum(grad_gate * lagged(up_values, tap_count - 1 - tap_index, position), axis=0)
                for tap_index in range(tap_count)
            ],
            axis=0,
        )
        * grad_scale
    )
    bias_terms = jnp.sum(grad_gate, axis=0) * grad_scale
    grad_rows = lax.psum_scatter(
        lax.dot_general(
            x_prev, grad_up, (((0,), (0,)), ((), ())), preferred_element_type=jnp.float32
        )
        * grad_scale,
        "fs",
        scatter_dimension=0,
        tiled=True,
    )
    tap_terms, bias_terms = lax.psum((tap_terms, bias_terms), "fs")
    grad_rows, tap_terms, bias_terms = lax.psum((grad_rows, tap_terms, bias_terms), "rep")
    return (
        hidden_next,
        grad_input,
        grad_value,
        sum_w + grad_rows,
        sum_taps + tap_terms,
        sum_bias + bias_terms,
    )


def solution(mesh):
    in_specs = (
        P(("rep", "fs"), None),
        P(("rep", "fs"), "tp"),
        P(("rep", "fs"), None),
        P(("rep", "fs"), "tp"),
        P(("rep", "fs"), "tp"),
        P("fs", "tp"),
        P(None, "tp"),
        P("tp"),
        P("fs", "tp"),
        P(None, "tp"),
        P("tp"),
    )
    out_specs = (
        P(("rep", "fs"), "tp"),
        P(("rep", "fs"), None),
        P(("rep", "fs"), "tp"),
        P("fs", "tp"),
        P(None, "tp"),
        P("tp"),
    )
    return jax.shard_map(
        per_device, mesh=mesh, in_specs=in_specs, out_specs=out_specs, check_vma=False
    )
```

profile of v0, /device:TPU:0, one launch (start us, length us, event | category | flops | bytes accessed | tf_op | source)
XLA Modules:
  0.0 426.5 jit_solution(13069589023482177257)
XLA Ops:
  7.2 0.7 all-gather.2.cloned.1.call-update
  8.0 0.9 slice_reduce_fusion.2
  8.9 102.7 %all-gather.2.cloned.1.call-done = bf16[2048,1536]{1,0:T(8,128)(2,1)} async-done(((bf16[256,1536]{1,0:T(8,128)(2,1)}), bf16[2048,1536]{1,0:T(8,128)(2,1)}) %all-gather.2.cloned.1.call-update) | async-done | bytes 6291472 | tf_op jit(solution)/shard_map/all_gather | solution.py:53
  111.6 4.8 %fusion = f32[384,1536]{1,0:T(8,128)S(1)} fusion(bf16[384,2048]{1,0:T(8,128)(2,1)S(1)} %copy-done, bf16[2048,1536]{1,0:T(8,128)(2,1)} %all-gather.2.cloned.1.call-done), kind=kOutput, calls=%fused_computation.5 | convolution fusion | flops 2417098752 | bytes 10223616 | tf_op jit(solution)/shard_map/dot_general | solution.py:55
  116.5 0.2 copy-done.8
  116.7 2.6 fusion.1
  119.3 6.6 %fusion.15 = (f32[1536]{0:T(1024)S(1)}, f32[1536]{0:T(1024)S(1)}, f32[1536]{0:T(1024)S(1)}, f32[1536]{0:T(1024)S(1)}, f32[384,1536]{1,0:T(8,128)S(1)}, /*index=5*/f32[384,1536]{1,0:T(8,128)}, bf16[384,1536]{1,0:T(8,128)(2,1)}) fusion(f32[384,1536]{1,0:T(8,128)S(1)} %fusion, pred[384]{0:T(512)(128)(4,1)S(1)} %get-tuple-element.26, ...), kind=kLoop, calls=%fused_computation.37 | loop fusion | flops 25356288 | bytes 23606400 | tf_op jit(solution)/shard_map/reduce_sum | solution.py:97
  126.0 0.2 slice.49
  126.2 0.2 slice.48
  126.5 1.3 add_convert_fusion
  127.7 6.5 %multiply_bitcast_fusion = f32[2048,1536]{0,1:T(8,128)} fusion(bf16[384,1536]{1,0:T(8,128)(2,1)S(1)} %add_convert_fusion, bf16[384,2048]{1,0:T(8,128)(2,1)S(1)} %copy-done), kind=kOutput, calls=%fused_computation | convolution fusion | flops 2419064832 | bytes 15335424 | tf_op jit(solution)/shard_map/dot_general | solution.py:99
  134.2 0.0 all-reduce.13.cloned.1.call-start
  134.3 206.1 %reduce-scatter.2.cloned.1.call-done = f32[256,1536]{0,1:T(8,128)} async-done(((f32[2048,1536]{0,1:T(8,128)}), f32[256,1536]{0,1:T(8,128)}) %reduce-scatter.2.cloned.1.call-update) | async-done | bytes 1572880 | tf_op jit(solution)/shard_map/reduce_scatter | solution.py:98
  340.4 8.1 %convolution_convert_fusion = bf16[384,2048]{1,0:T(8,128)(2,1)} fusion(bf16[384,1536]{1,0:T(8,128)(2,1)S(1)} %add_convert_fusion, bf16[2048,1536]{1,0:T(8,128)(2,1)} %all-gather.2.cloned.1.call-done), kind=kOutput, calls=%fused_computation.3 | convolution fusion | flops 2416705536 | bytes 9043968 | tf_op jit(solution)/shard_map/dot_general | solution.py:79
  348.5 1.9 copy.17
  350.5 35.5 %all-reduce.6 = (f32[3,1536]{1,0:T(4,128)S(1)}, f32[1536]{0:T(1024)S(1)}) all-reduce(f32[3,1536]{1,0:T(4,128)S(1)} %maximum_multiply_fusion, f32[1536]{0:T(1024)S(1)} %broadcast_multiply_fusion), channel_id=1, replica_groups=mesh['rep'=2,'fs'=8,'tp'=2] {'fs'}, use_global_device_ids=true, to_apply=%region_6.7 | all-reduce | flops 6144 | bytes 49152 | tf_op jit(solution)/shard_map/psum | solution.py:107
  386.0 8.8 %all-reduce.7 = (f32[3,1536]{1,0:T(4,128)S(1)}, f32[1536]{0:T(1024)S(1)}) all-reduce(f32[3,1536]{1,0:T(4,128)S(1)} %get-tuple-element.19, f32[1536]{0:T(1024)S(1)} %get-tuple-element.20), channel_id=1, replica_groups=mesh['rep'=2,'fs'=8,'tp'=2] {'rep'}, use_global_device_ids=true, to_apply=%region_7.8 | all-reduce | flops 6144 | bytes 49152 | tf_op jit(solution)/shard_map/psum | solution.py:108
  394.9 0.6 add.131
  395.5 0.6 add.132
  396.1 3.6 fusion.5
  399.7 2.7 add.130
  402.4 3.1 copy.18
  405.5 11.6 %all-reduce.11.cloned.1.call-done = bf16[384,2048]{1,0:T(8,128)(2,1)} async-done(((bf16[384,2048]{1,0:T(8,128)(2,1)}), bf16[384,2048]{1,0:T(8,128)(2,1)}) %all-reduce.11.cloned.1.call-update) | async-done | bytes 1572880 | tf_op jit(solution)/shard_map/psum | solution.py:82
  417.2 2.7 copy.21
  (33 shorter events, 0.3 us)
Async XLA Ops:
  7.2 104.5 %copy-start = (bf16[384,2048]{1,0:T(8,128)(2,1)S(1)}, bf16[384,2048]{1,0:T(8,128)(2,1)}, u32[]{:S(2)}) copy-start(bf16[384,2048]{1,0:T(8,128)(2,1)} %param.13) | copy-start | bytes 4718596
  7.2 104.4 %all-gather.2.cloned.1.call-start = ((), (), s32[]{:S(2)}) async-start(), calls=%async_computation.1 | async-start | bytes 7077888 | tf_op jit(solution)/shard_map/all_gather | solution.py:53
  7.9 332.5 %reduce-scatter.2.cloned.1.call-start = ((), (), s32[]{:S(2)}) async-start(), calls=%async_computation.3 | async-start | bytes 14155776 | tf_op jit(solution)/shard_map/reduce_scatter | solution.py:98
  111.6 4.8 %copy-start.7 = (bf16[2048,1536]{1,0:T(8,128)(2,1)S(1)}, bf16[2048,1536]{1,0:T(8,128)(2,1)}, u32[]{:S(2)}) copy-start(bf16[2048,1536]{1,0:T(8,128)(2,1)} %all-gather.2.cloned.1.call-done) | copy-start | bytes 18874372
  111.6 5.1 %copy-start.8 = (bf16[384,2048]{1,0:T(8,128)(2,1)S(1)}, bf16[384,2048]{1,0:T(8,128)(2,1)}, u32[]{:S(2)}) copy-start(bf16[384,2048]{1,0:T(8,128)(2,1)} %param.11) | copy-start | bytes 4718596
  116.7 2.6 copy-start.1
  116.7 2.6 copy-start.2
  116.7 2.6 copy-start.3
  116.7 2.6 copy-start.5
  134.2 265.5 %all-reduce.13.cloned.1.call-start = ((), (), s32[]{:S(2)}) async-start(), calls=%async_computation.4 | async-start | bytes 3145728 | tf_op jit(solution)/shard_map/psum | solution.py:108
  340.4 76.8 %all-reduce.11.cloned.1.call-start = ((), (), s32[]{:S(2)}) async-start(), calls=%async_computation.2 | async-start | bytes 3145728 | tf_op jit(solution)/shard_map/psum | solution.py:82
  348.5 46.3 %copy-start.4 = (f32[3,1536]{1,0:T(4,128)S(1)}, f32[3,1536]{1,0:T(4,128)}, u32[]{:S(2)}) copy-start(f32[3,1536]{1,0:T(4,128)} %param.20) | copy-start | bytes 55300
  348.5 47.0 %copy-start.6 = (f32[1536]{0:T(1024)S(1)}, f32[1536]{0:T(1024)}, u32[]{:S(2)}) copy-start(f32[1536]{0:T(1024)} %param.21) | copy-start | bytes 18436
Sparse Core Ops, SparseCore 0:
  10.2 101.4 all-gather.1
  134.3 205.9 reduce-scatter.1
  342.7 51.1 all-reduce.12
  396.6 20.5 all-reduce.10
where the time goes:
time: 427 us; the launch traced here: 426 us
  waiting for transfers between devices  321 us (75%)
  blocking collectives  44.3 us (10%)
  matrix products  21.9 us (5%)
  other arithmetic  15.5 us (4%)
  between operations  14 us (3%)
  local copies, waits for them, and re-layouts  9.38 us (2%)
    reduce_scatter x1, waiting for transfers between devices, per_device(): lax.psum_scatter(lax.dot_general(x_prev, grad_up, (((0,), (0,)), ((), ())...  206 us
    all_gather x1, waiting for transfers between devices, per_device(): gathered = lax.all_gather(w_gate, 'fs', axis=0, tiled=True)  103 us
    psum x1, blocking collectives, per_device(): tap_terms, bias_terms = lax.psum((tap_terms, bias_terms), 'fs')  35.5 us
    psum x1, waiting for transfers between devices, per_device(): grad_input = lax.psum(partial_input.astype(jnp.bfloat16), 'tp')  11.6 us
    psum x1, blocking collectives, per_device(): lax.psum((grad_rows, tap_terms, bias_terms), 'rep')  8.82 us
  transfers between devices with their start and end apart: 4, of which 3 were waited for; matrix products, arithmetic and copies ran while one was open for 5% of the time, Pallas kernels for 0%

commit v1 on v0

--- a/solution.py
+++ b/solution.py
@@ -1,9 +1,16 @@
+import functools
+
 import jax
 import jax.numpy as jnp
 from jax import lax
+from jax.experimental import pallas as pl
+from jax.experimental.pallas import tpu as pltpu
 from jax.sharding import PartitionSpec as P
 
 SEQ_LEN = 128
+MESH = pl.DeviceIdType.MESH
+VMEM = pltpu.VMEM
+IN_VMEM = pl.BlockSpec(memory_space=pltpu.VMEM)
 
 
 def lagged(values, offset, position):
@@ -32,6 +39,307 @@
             values, tap_count - 1 - tap_index, position
         )
     return result
+
+
+def ring_spot(index, count):
+    pair, odd = lax.div(index, 2), lax.rem(index, 2)
+    return pair * (1 - odd) + (count - 1 - pair) * odd
+
+
+def ring_member(spot, count):
+    down = lax.div(spot, count // 2)
+    return 2 * spot * (1 - down) + (2 * (count - 1 - spot) + 1) * down
+
+
+def greet(devices):
+    barrier = pltpu.get_barrier_semaphore()
+    for device in devices:
+        pl.semaphore_signal(barrier, inc=1, device_id=device, device_id_type=MESH)
+    pl.semaphore_wait(barrier, len(devices))
+
+
+def remote(source, target, send, recv, device):
+    return pltpu.make_async_remote_copy(
+        src_ref=source,
+        dst_ref=target,
+        send_sem=send,
+        recv_sem=recv,
+        device_id=device,
+        device_id_type=MESH,
+    )
+
+
+def piece_rows(rep, quarter):
+    own = pl.multiple_of(rep * (3 * quarter), quarter)
+    return (pl.ds(own, quarter), pl.ds(quarter, quarter), pl.ds(2 * quarter, quarter))
+
+
+def gather_kernel(count, w_ref, out_ref, ring_send, ring_recv, side_send, side_recv):
+    fs, rep = lax.axis_index("fs"), lax.axis_index("rep")
+    half = count // 2
+    rows = piece_rows(rep, w_ref.shape[0] // 4)
+    spot = ring_spot(fs, count)
+
+    def at(offset):
+        return ring_member(lax.rem(spot + offset + count, count), count)
+
+    toward = ({"fs": at(1)}, {"fs": at(-1)})
+    across = {"rep": 1 - rep}
+    greet((*toward, across))
+
+    def parts(way, step):
+        return (0, 1, 2) if step < half else ((0, 1), (2,))[way]
+
+    def hop(way, step, piece):
+        owner = at((1 - step, step - 1)[way])
+        block = w_ref.at[rows[piece]] if step == 1 else out_ref.at[owner, rows[piece]]
+        sems = (way, step - 1, piece)
+        return remote(
+            block, out_ref.at[owner, rows[piece]], ring_send.at[sems], ring_recv.at[sems], toward[way]
+        )
+
+    def side(way, step):
+        block = out_ref.at[at((-step, step)[way]), rows[0]]
+        sems = (way, step - 1)
+        return remote(block, block, side_send.at[sems], side_recv.at[sems], across)
+
+    hops, sides = [], []
+    for piece in range(3):
+        for way in range(2):
+            hops.append(hop(way, 1, piece))
+            hops[-1].start()
+    out_ref[fs] = w_ref[...]
+    for step in range(1, half + 1):
+        for piece in range(3):
+            for way in range(2):
+                if piece not in parts(way, step):
+                    continue
+                hop(way, step, piece).wait_recv()
+                if step < half and piece in parts(way, step + 1):
+                    hops.append(hop(way, step + 1, piece))
+                    hops[-1].start()
+                if piece == 0:
+                    sides.append(side(way, step))
+                    sides[-1].start()
+    for copy in hops:
+        copy.wait_send()
+    for copy in sides:
+        copy.wait()
+
+
+def gather_weight(w_gate, count):
+    depth, columns = w_gate.shape
+    return pl.pallas_call(
+        functools.partial(gather_kernel, count),
+        out_shape=jax.ShapeDtypeStruct((count, depth, columns), w_gate.dtype),
+        in_specs=[IN_VMEM],
+        out_specs=IN_VMEM,
+        scratch_shapes=[
+            pltpu.SemaphoreType.DMA((2, count // 2, 3)),
+            pltpu.SemaphoreType.DMA((2, count // 2, 3)),
+            pltpu.SemaphoreType.DMA((2, count // 2)),
+            pltpu.SemaphoreType.DMA((2, count // 2)),
+        ],
+        compiler_params=pltpu.CompilerParams(
+            collective_id=0, has_side_effects=True, vmem_limit_bytes=40 * 2**20
+        ),
+        name="gather_weight",
+    )(w_gate)
+
+
+def reduce_kernel(
+    count,
+    peers,
+    grad_ref,
+    term_ref,
+    part_ref,
+    total_ref,
+    terms_ref,
+    parts_ref,
+    side_buf,
+    out_buf,
+    in_buf,
+    last_out,
+    last_in,
+    term_in,
+    term_buf,
+    side_send,
+    side_recv,
+    ring_send,
+    ring_recv,
+    last_send,
+    last_recv,
+    term_send,
+    term_recv,
+    pair_send,
+    pair_recv,
+    peer_send,
+    peer_recv,
+):
+    fs, rep, tp = lax.axis_index("fs"), lax.axis_index("rep"), lax.axis_index("tp")
+    half = count // 2
+    quarter = grad_ref.shape[1] // 4
+    rows, other_rows = piece_rows(rep, quarter), piece_rows(1 - rep, quarter)[0]
+    spot = ring_spot(fs, count)
+
+    def at(offset):
+        return ring_member(lax.rem(spot + offset + count, count), count)
+
+    toward = ({"fs": at(1)}, {"fs": at(-1)})
+    across = {"rep": 1 - rep}
+    others = [{"tp": lax.rem(tp + shift, peers)} for shift in range(1, peers)]
+    greet((*toward, across, *others))
+
+    pair = remote(term_ref, term_in, pair_send.at[0], pair_recv.at[0], across)
+    pair.start()
+    spread = [
+        remote(part_ref, parts_ref.at[tp], peer_send.at[i], peer_recv.at[i], device)
+        for i, device in enumerate(others)
+    ]
+    for copy in spread:
+        copy.start()
+
+    def side(offset):
+        slot = offset % count
+        owner = at(offset)
+        return remote(
+            grad_ref.at[owner, other_rows],
+            side_buf.at[slot],
+            side_send.at[slot],
+            side_recv.at[slot],
+            across,
+        )
+
+    order = [half] + [sign * k for k in range(half - 1, 0, -1) for sign in (1, -1)] + [0]
+    sides = [side(offset) for offset in order]
+    for copy in sides:
+        copy.start()
+
+    def parts(way, step):
+        return (0, 1, 2) if step > 1 else ((0, 1), (2,))[way]
+
+    def hop(way, step, piece):
+        sems = (way, step - 1, piece)
+        return remote(
+            out_buf.at[sems], in_buf.at[sems], ring_send.at[sems], ring_recv.at[sems], toward[way]
+        )
+
+    def own(offset, piece):
+        values = grad_ref[at(offset), rows[piece]].astype(jnp.float32)
+        if piece == 0:
+            values = values + side_buf[offset % count].astype(jnp.float32)
+        return values
+
+    hops = []
+
+    def send(way, step, piece, fresh):
+        offset = (half - step + 1) * (1, -1)[way]
+        if piece == 0 and (way == 0 or step > 1):
+            side(offset).wait_recv()
+        values = own(offset, piece)
+        if not fresh:
+            values = values + in_buf[way, step - 2, piece].astype(jnp.float32)
+        out_buf[way, step - 1, piece] = values.astype(out_buf.dtype)
+        hops.append(hop(way, step, piece))
+        hops[-1].start()
+
+    def term_hop(way, step):
+        block = term_buf.at[at((1 - step, step - 1)[way])]
+        sems = (way, step - 1)
+        return remote(block, block, term_send.at[sems], term_recv.at[sems], toward[way])
+
+    for way, step, piece in ((0, 1, 1), (1, 1, 2), (0, 2, 2), (1, 2, 1)):
+        send(way, step, piece, True)
+    parts_ref[tp] = part_ref[...]
+    pair.wait()
+    term_buf[fs] = term_ref[...] + term_in[...]
+    term_hops = [term_hop(way, 1) for way in range(2)]
+    for copy in term_hops:
+        copy.start()
+    send(0, 1, 0, True)
+    send(1, 2, 0, True)
+    for step in range(1, half):
+        for piece in (1, 2, 0):
+            for way in range(2):
+                if piece in parts(way, step):
+                    hop(way, step, piece).wait_recv()
+                    send(way, step + 1, piece, False)
+        for way in range(2):
+            term_hop(way, step).wait_recv()
+            if step + 1 < half or way == 0:
+                term_hops.append(term_hop(way, step + 1))
+                term_hops[-1].start()
+    lasts = {}
+    side(0).wait_recv()
+    for piece in (1, 2, 0):
+        values = own(0, piece)
+        for way in range(2):
+            hop(way, half, piece).wait_recv()
+            values = values + in_buf[way, half - 1, piece].astype(jnp.float32)
+        last_out[piece] = values.astype(last_out.dtype)
+        lasts[piece] = remote(
+            last_out.at[piece], last_in.at[piece], last_send.at[piece], last_recv.at[piece], across
+        )
+        lasts[piece].start()
+    term_hop(0, half).wait_recv()
+    terms = term_buf[0]
+    for index in range(1, count):
+        terms = terms + term_buf[index]
+    terms_ref[...] = terms
+    for piece in (1, 2):
+        lasts[piece].wait_recv()
+        total_ref[rows[piece]] = last_out[piece].astype(jnp.float32) + last_in[piece].astype(
+            jnp.float32
+        )
+    total_ref[rows[0]] = last_out[0].astype(jnp.float32)
+    lasts[0].wait_recv()
+    total_ref[other_rows] = last_in[0].astype(jnp.float32)
+    for copy in (*sides, *hops, *term_hops, *lasts.values()):
+        copy.wait_send()
+    for copy in spread:
+        copy.wait()
+
+
+def reduce_gradients(grad_blocks, terms, part, peers):
+    count, depth, columns = grad_blocks.shape
+    half, quarter = count // 2, depth // 4
+    dma = pltpu.SemaphoreType.DMA
+    pieces = (2, half, 3)
+    return pl.pallas_call(
+        functools.partial(reduce_kernel, count, peers),
+        out_shape=(
+            jax.ShapeDtypeStruct((depth, columns), jnp.float32),
+            jax.ShapeDtypeStruct(terms.shape, jnp.float32),
+            jax.ShapeDtypeStruct((peers, *part.shape), part.dtype),
+        ),
+        in_specs=[IN_VMEM] * 3,
+        out_specs=(IN_VMEM,) * 3,
+        scratch_shapes=[
+            VMEM((count, quarter, columns), jnp.bfloat16),
+            VMEM((*pieces, quarter, columns), jnp.bfloat16),
+            VMEM((*pieces, quarter, columns), jnp.bfloat16),
+            VMEM((3, quarter, columns), jnp.bfloat16),
+            VMEM((3, quarter, columns), jnp.bfloat16),
+            VMEM(terms.shape, jnp.float32),
+            VMEM((count, *terms.shape), jnp.float32),
+            dma((count,)),
+            dma((count,)),
+            dma(pieces),
+            dma(pieces),
+            dma((3,)),
+            dma((3,)),
+            dma((2, half)),
+            dma((2, half)),
+            dma((1,)),
+            dma((1,)),
+            dma((peers,)),
+            dma((peers,)),
+        ],
+        compiler_params=pltpu.CompilerParams(
+            collective_id=1, has_side_effects=True, vmem_limit_bytes=56 * 2**20
+        ),
+        name="reduce_gradients",
+    )(grad_blocks, terms, part)
 
 
 def per_device(
@@ -50,7 +358,8 @@
     row_count = x_next.shape[0]
     tap_count = conv_taps.shape[0]
     position = jnp.arange(row_count) % SEQ_LEN
-    gathered = lax.all_gather(w_gate, "fs", axis=0, tiled=True)
+    fs_count = lax.axis_size("fs")
+    gathered = gather_weight(w_gate, fs_count).reshape(fs_count * w_gate.shape[0], w_gate.shape[1])
     up_next = jnp.dot(x_next, gathered, preferred_element_type=jnp.float32)
     up_prev = jnp.dot(x_prev, gathered, preferred_element_type=jnp.float32)
     up_next = up_next.astype(jnp.bfloat16)
@@ -79,40 +388,33 @@
     partial_input = lax.dot_general(
         grad_up, gathered, contract_units, preferred_element_type=jnp.float32
     )
-    grad_input = lax.psum(partial_input.astype(jnp.bfloat16), "tp")
     rep_count = lax.axis_size("rep")
-    fs_count = lax.axis_size("fs")
     grad_scale = float(row_count * rep_count * fs_count) ** (-0.5)
     up_values = up_prev.astype(jnp.float32)
-    tap_terms = (
-        jnp.stack(
-            [
-                jnp.sum(grad_gate * lagged(up_values, tap_count - 1 - tap_index, position), axis=0)
-                for tap_index in range(tap_count)
-            ],
-            axis=0,
-        )
-        * grad_scale
-    )
-    bias_terms = jnp.sum(grad_gate, axis=0) * grad_scale
-    grad_rows = lax.psum_scatter(
-        lax.dot_general(
-            x_prev, grad_up, (((0,), (0,)), ((), ())), preferred_element_type=jnp.float32
-        )
-        * grad_scale,
-        "fs",
-        scatter_dimension=0,
-        tiled=True,
-    )
-    tap_terms, bias_terms = lax.psum((tap_terms, bias_terms), "fs")
-    grad_rows, tap_terms, bias_terms = lax.psum((grad_rows, tap_terms, bias_terms), "rep")
+    terms = jnp.stack(
+        [
+            jnp.sum(grad_gate * lagged(up_values, tap_count - 1 - tap_index, position), axis=0)
+            for tap_index in range(tap_count)
+        ]
+        + [jnp.sum(grad_gate, axis=0)],
+        axis=0,
+    )
+    grad_blocks = (
+        lax.dot_general(x_prev, grad_up, (((0,), (0,)), ((), ())), preferred_element_type=jnp.float32)
+        .astype(jnp.bfloat16)
+        .reshape(fs_count, *w_gate.shape)
+    )
+    grad_rows, terms, partials = reduce_gradients(
+        grad_blocks, terms, partial_input.astype(jnp.bfloat16), lax.axis_size("tp")
+    )
+    grad_input = jnp.sum(partials.astype(jnp.float32), axis=0).astype(jnp.bfloat16)
     return (
         hidden_next,
         grad_input,
         grad_value,
-        sum_w + grad_rows,
-        sum_taps + tap_terms,
-        sum_bias + bias_terms,
+        sum_w + grad_scale * grad_rows,
+        sum_taps + grad_scale * terms[:tap_count],
+        sum_bias + grad_scale * terms[tap_count],
     )
 
 

time: 427 us -> 163 us (0.38)
  waiting for transfers between devices: 321 us -> 0 us
  Pallas kernels: 0 us -> 117 us
  blocking collectives: 44.3 us -> 0 us
  between operations: 14 us -> 0.9 us
  matrix products: 21.9 us -> 14.3 us
    reduce_scatter x1 -> x0, waiting for transfers between devices: 206 us -> none  [per_device(): lax.psum_scatter(lax.dot_general(x_prev, grad_up, (((0,), (0,)), ((), ())...]
    pallas_call x0 -> x2, Pallas kernels: none -> 117 us  [the longest x1 63.3 us: reduce_gradients(): pl.pallas_call(functools.partial(reduce_kernel, count, peers), out_shape=...]
    all_gather x1 -> x0, waiting for transfers between devices: 103 us -> none  [per_device(): gathered = lax.all_gather(w_gate, 'fs', axis=0, tiled=True)]
    psum x2 -> x0, blocking collectives: 44.3 us -> none  [the longest x1 35.5 us: per_device(): tap_terms, bias_terms = lax.psum((tap_terms, bias_terms), 'fs')]
    psum x2 -> x0, waiting for transfers between devices: 11.6 us -> none  [the longest x1 11.6 us: per_device(): grad_input = lax.psum(partial_input.astype(jnp.bfloat16), 'tp')]
    convert_element_type x0 -> x1, local copies, waits for them, and re-layouts: none -> 8.67 us  [per_device(): grad_blocks = lax.dot_general(x_prev, grad_up, (((0,), (0,)), ((), ())),...]
    unnamed x21 -> x22, local copies, waits for them, and re-layouts: 7.96 us -> 1.19 us
    dot_general x1, matrix products: 8.05 us -> 3.75 us  [per_device(): lax.dot_general(grad_up, gathered, contract_units, preferred_element_type...]
  transfers between devices with their start and end apart: 4 -> 0, of which waited for: 3 -> 0; matrix products, arithmetic and copies ran while one was open for 5% -> 0% of each run, Pallas kernels for 0% -> 0%
where the time goes in v1:
time: 163 us
  Pallas kernels  117 us (72%)
  other arithmetic  19.2 us (12%)
  matrix products  14.3 us (9%)
  local copies, waits for them, and re-layouts  11.3 us (7%)
    pallas_call x1, Pallas kernels, reduce_gradients(): pl.pallas_call(functools.partial(reduce_kernel, count, peers), out_shape=...  63.3 us
    pallas_call x1, Pallas kernels, gather_weight(): pl.pallas_call(functools.partial(gather_kernel, count), out_shape=jax.Sha...  53.9 us
    convert_element_type x1, local copies, waits for them, and re-layouts, per_device(): grad_blocks = lax.dot_general(x_prev, grad_up, (((0,), (0,)), ((), ())),...  8.67 us
    convert_element_type x1, other arithmetic, per_device(): grad_value = (cot_values * gate_prev * sigmoid_gate).astype(jnp.bfloat16)  5.86 us
    dot_general x1, matrix products, per_device(): lax.dot_general(x_prev, grad_up, (((0,), (0,)), ((), ())), preferred_elem...  5.35 us
    reduce_sum x1, other arithmetic, per_device(): jnp.sum(partials.astype(jnp.float32), axis=0).astype(jnp.bfloat16)  4.33 us
    dot_general x1, matrix products, per_device(): lax.dot_general(grad_up, gathered, contract_units, preferred_element_type...  3.75 us

profile of v1, /device:TPU:0, one launch (start us, length us, event | category | flops | bytes accessed | tf_op | source)
XLA Modules:
  0.0 162.9 jit_solution(1269300347413355135)
XLA Ops:
  0.6 0.0 copy-start
  0.7 0.9 slice_reduce_fusion.2
  1.6 0.0 copy-start.1
  1.6 1.1 copy-done.1
  2.8 53.9 %gather_weight.1 = bf16[8,256,1536]{2,1,0:T(8,128)(2,1)S(1)} custom-call(bf16[256,1536]{1,0:T(8,128)(2,1)S(1)} %copy-done.1), custom_call_target="tpu_custom_call" | custom-call | tf_op jit(solution)/shard_map/gather_weight/pallas_call | solution.py:132
  56.7 0.0 copy-start.10
  56.7 2.6 %fusion.1 = f32[384,1536]{1,0:T(8,128)S(1)} fusion(bf16[384,2048]{1,0:T(8,128)(2,1)S(1)} %copy-done, bf16[2048,1536]{1,0:T(8,128)(2,1)S(1)} %bitcast.16), kind=kOutput, calls=%fused_computation.6 | convolution fusion | flops 2417098752 | bytes 10223616 | tf_op jit(solution)/shard_map/dot_general | solution.py:364
  59.3 0.0 copy-start.2
  59.4 2.6 %fusion.2 = f32[384,1536]{1,0:T(8,128)S(1)} fusion(bf16[384,2048]{1,0:T(8,128)(2,1)S(1)} %copy-done.10, bf16[2048,1536]{1,0:T(8,128)(2,1)S(1)} %bitcast.17), kind=kOutput, calls=%fused_computation.8 | convolution fusion | flops 2417098752 | bytes 10223616 | tf_op jit(solution)/shard_map/dot_general | solution.py:363
  62.1 5.9 %fusion.6 = (bf16[384,1536]{1,0:T(8,128)(2,1)}, f32[384,1536]{1,0:T(8,128)S(1)}, bf16[384,1536]{1,0:T(8,128)(2,1)}) fusion(bf16[384,1536]{1,0:T(8,128)(2,1)S(1)} %copy-done.2, f32[384,1536]{1,0:T(8,128)S(1)} %fusion.1, pred[384]{0:T(512)(128)(4,1)S(1)} %get-tuple-element.23, f32[1536]{0:T(1024)S(1)} %get-tuple-element.17, f32[383,1536]{1,0:T(8,128)S(1)} %bitcast.19, ...), kind=kLoop, calls=%fused_computation.12 | loop fusion | flops 18874368 | bytes 21222528 | tf_op jit(solution)/shard_map/convert_element_type | solution.py:374
  67.9 3.1 %multiply_reduce_fusion.2 = (f32[1536]{0:T(1024)S(1)}, f32[1536]{0:T(1024)S(1)}, f32[1536]{0:T(1024)S(1)}, f32[1536]{0:T(1024)S(1)}, f32[384,1536]{1,0:T(8,128)S(1)}) fusion(f32[382,1536]{1,0:T(8,128)S(1)} %bitcast.22, pred[384]{0:T(512)(128)(4,1)S(1)} %fusion.14, f32[384,1536]{1,0:T(8,128)S(1)} %fusion.1, pred[384]{0:T(512)(128)(4,1)S(1)} %get-tuple-element.23, ...), kind=kLoop, calls=%fused_computation.15 | loop fusion | flops 12380160 | bytes 14163072 | tf_op jit(solution)/shard_map/reduce_sum | solution.py:396
  71.0 0.6 pad_maximum_fusion.term_ref
  71.7 0.2 slice.57
  71.9 0.2 slice.56
  72.2 1.3 add_convert_fusion
  73.4 3.7 %convolution_convert_fusion.1.part_ref = bf16[384,2048]{1,0:T(8,128)(2,1)} fusion(bf16[384,1536]{1,0:T(8,128)(2,1)S(1)} %add_convert_fusion, bf16[2048,1536]{1,0:T(8,128)(2,1)S(1)} %bitcast.18), kind=kOutput, calls=%fused_computation.4 | convolution fusion | flops 2416705536 | bytes 9043968 | tf_op jit(solution)/shard_map/dot_general | solution.py:388
  77.2 5.3 %fusion = bf16[2048,1536]{0,1:T(8,128)(2,1)} fusion(bf16[384,1536]{1,0:T(8,128)(2,1)S(1)} %add_convert_fusion, bf16[384,2048]{1,0:T(8,128)(2,1)S(1)} %copy-done), kind=kOutput, calls=%fused_computation.1 | convolution fusion | flops 2419064832 | bytes 9043968 | tf_op jit(solution)/shard_map/dot_general | solution.py:403
  82.5 8.7 %copy.17 = bf16[2048,1536]{1,0:T(8,128)(2,1)} copy(bf16[2048,1536]{0,1:T(8,128)(2,1)} %fusion) | data formatting | bytes 12582912 | tf_op jit(solution)/shard_map/convert_element_type | solution.py:404
  91.2 63.3 %reduce_gradients.1 = (f32[256,1536]{1,0:T(8,128)}, f32[4,1536]{1,0:T(4,128)}, bf16[2,384,2048]{2,1,0:T(8,128)(2,1)}) custom-call(bf16[8,256,1536]{2,1,0:T(8,128)(2,1)} %bitcast.23, f32[4,1536]{1,0:T(4,128)} %pad_maximum_fusion.term_ref, bf16[384,2048]{1,0:T(8,128)(2,1)} %convolution_convert_fusion.1.part_ref), custom_call_target="tpu_custom_call" | custom-call | tf_op jit(solution)/shard_map/reduce_gradients/pallas_call | solution.py:308
  154.5 0.0 copy-start.7
  154.6 4.3 %reduce_sum.52 = bf16[384,2048]{1,0:T(8,128)(2,1)} reduce(bf16[2,384,2048]{2,1,0:T(8,128)(2,1)} %get-tuple-element.9, bf16[]{:T(256)} %constant.36.clone.1), dimensions={0}, to_apply=%region_4.5 | reduce | flops 786432 | bytes 4718594 | tf_op jit(solution)/shard_map/reduce_sum | solution.py:410
  158.9 0.6 multiply_add_fusion.2
  159.5 0.6 add.118
  160.1 2.8 %multiply_add_fusion.1 = f32[256,1536]{1,0:T(8,128)} fusion(f32[256,1536]{1,0:T(8,128)S(1)} %copy-done.3, f32[256,1536]{1,0:T(8,128)} %get-tuple-element.10), kind=kLoop, calls=%fused_computation.22 | loop fusion | flops 786432 | bytes 4718592 | tf_op jit(solution)/shard_map/add | solution.py:415
  (25 shorter events, 0.1 us)
Async XLA Ops:
  0.6 56.1 %copy-start = (bf16[384,2048]{1,0:T(8,128)(2,1)S(1)}, bf16[384,2048]{1,0:T(8,128)(2,1)}, u32[]{:S(2)}) copy-start(bf16[384,2048]{1,0:T(8,128)(2,1)} %param.13) | copy-start | bytes 4718596
  1.6 1.1 copy-start.1
  56.7 2.6 %copy-start.10 = (bf16[384,2048]{1,0:T(8,128)(2,1)S(1)}, bf16[384,2048]{1,0:T(8,128)(2,1)}, u32[]{:S(2)}) copy-start(bf16[384,2048]{1,0:T(8,128)(2,1)} %param.11) | copy-start | bytes 4718596
  59.3 2.7 %copy-start.2 = (bf16[384,1536]{1,0:T(8,128)(2,1)S(1)}, bf16[384,1536]{1,0:T(8,128)(2,1)}, u32[]{:S(2)}) copy-start(bf16[384,1536]{1,0:T(8,128)(2,1)} %param.15) | copy-start | bytes 3538948
  59.4 2.7 %copy-start.4 = (bf16[384,1536]{1,0:T(8,128)(2,1)S(1)}, bf16[384,1536]{1,0:T(8,128)(2,1)}, u32[]{:S(2)}) copy-start(bf16[384,1536]{1,0:T(8,128)(2,1)} %param.12) | copy-start | bytes 3538948
  59.4 2.7 %copy-start.8 = (f32[1536]{0:T(1024)S(1)}, f32[1536]{0:T(1024)}, u32[]{:S(2)}) copy-start(f32[1536]{0:T(1024)} %param.18) | copy-start | bytes 18436
  62.0 5.9 %copy-start.5 = (bf16[384,1536]{1,0:T(8,128)(2,1)S(1)}, bf16[384,1536]{1,0:T(8,128)(2,1)}, u32[]{:S(2)}) copy-start(bf16[384,1536]{1,0:T(8,128)(2,1)} %param.14) | copy-start | bytes 3538948
  154.5 4.4 %copy-start.6 = (f32[4,1536]{1,0:T(4,128)S(1)}, f32[4,1536]{1,0:T(4,128)}, u32[]{:S(2)}) copy-start(f32[4,1536]{1,0:T(4,128)} %get-tuple-element.11) | copy-start | bytes 73732
  154.5 4.4 %copy-start.7 = (f32[3,1536]{1,0:T(4,128)S(1)}, f32[3,1536]{1,0:T(4,128)}, u32[]{:S(2)}) copy-start(f32[3,1536]{1,0:T(4,128)} %param.20) | copy-start | bytes 55300
  154.5 5.0 %copy-start.9 = (f32[1536]{0:T(1024)S(1)}, f32[1536]{0:T(1024)}, u32[]{:S(2)}) copy-start(f32[1536]{0:T(1024)} %param.21) | copy-start | bytes 18436
  154.5 5.6 %copy-start.3 = (f32[256,1536]{1,0:T(8,128)S(1)}, f32[256,1536]{1,0:T(8,128)}, u32[]{:S(2)}) copy-start(f32[256,1536]{1,0:T(8,128)} %param.19) | copy-start | bytes 4718596

commit v2 on v1

--- a/solution.py
+++ b/solution.py
@@ -69,15 +69,35 @@
     )
 
 
-def piece_rows(rep, quarter):
-    own = pl.multiple_of(rep * (3 * quarter), quarter)
-    return (pl.ds(own, quarter), pl.ds(quarter, quarter), pl.ds(2 * quarter, quarter))
-
-
-def gather_kernel(count, w_ref, out_ref, ring_send, ring_recv, side_send, side_recv):
+def piece_rows(rep, depth, alone):
+    shared = (depth - 2 * alone) // 2
+    own = pl.multiple_of(rep * (depth - alone), 16)
+    return (pl.ds(own, alone), pl.ds(alone, shared), pl.ds(alone + shared, shared))
+
+
+def column_tile(columns):
+    return 512 if columns % 512 == 0 else columns
+
+
+def gather_kernel(
+    count,
+    w_ref,
+    x_next_ref,
+    x_prev_ref,
+    out_ref,
+    up_next_ref,
+    up_prev_ref,
+    sums,
+    ring_send,
+    ring_recv,
+    side_send,
+    side_recv,
+):
     fs, rep = lax.axis_index("fs"), lax.axis_index("rep")
     half = count // 2
-    rows = piece_rows(rep, w_ref.shape[0] // 4)
+    depth, columns = w_ref.shape
+    rows = piece_rows(rep, depth, max(1, 5 * depth // 256) * 16)
+    streamed, tile = depth % 128 == 0, column_tile(columns)
     spot = ring_spot(fs, count)
 
     def at(offset):
@@ -88,7 +108,21 @@
     greet((*toward, across))
 
     def parts(way, step):
-        return (0, 1, 2) if step < half else ((0, 1), (2,))[way]
+        return (0, 1, 2) if step < half else ((0,), (1, 2))[way]
+
+    def accumulate(offset):
+        owner = at(offset)
+        lanes = pl.ds(pl.multiple_of(owner * depth, 128), depth)
+
+        @pl.loop(0, columns // tile)
+        def _(index):
+            where = pl.ds(pl.multiple_of(index * tile, 128), tile)
+            block = out_ref[owner, :, where]
+            for branch, x_ref in enumerate((x_next_ref, x_prev_ref)):
+                product = jnp.dot(x_ref[:, lanes], block, preferred_element_type=jnp.float32)
+                if offset != 0:
+                    product = product + sums[branch, :, where]
+                sums[branch, :, where] = product
 
     def hop(way, step, piece):
         owner = at((1 - step, step - 1)[way])
@@ -121,20 +155,39 @@
                 if piece == 0:
                     sides.append(side(way, step))
                     sides[-1].start()
-    for copy in hops:
+        if streamed and step == 1:
+            accumulate(0)
+        elif streamed:
+            for way in range(2):
+                side(way, step - 1).wait_recv()
+                accumulate((1 - step, step - 1)[way])
+    side(0, half).wait_recv()
+    if streamed:
+        accumulate(half)
+        up_next_ref[...] = sums[0].astype(up_next_ref.dtype)
+        up_prev_ref[...] = sums[1].astype(up_prev_ref.dtype)
+    else:
+        for step in range(1, half):
+            for way in range(2):
+                side(way, step).wait_recv()
+        whole = out_ref[...].reshape(count * depth, columns)
+        for x_ref, up_ref in ((x_next_ref, up_next_ref), (x_prev_ref, up_prev_ref)):
+            up = jnp.dot(x_ref[...], whole, preferred_element_type=jnp.float32)
+            up_ref[...] = up.astype(up_ref.dtype)
+    for copy in (*hops, *sides):
         copy.wait_send()
-    for copy in sides:
-        copy.wait()
-
-
-def gather_weight(w_gate, count):
+
+
+def gather_weight(w_gate, x_next, x_prev, count):
     depth, columns = w_gate.shape
+    up = jax.ShapeDtypeStruct((x_next.shape[0], columns), jnp.bfloat16)
     return pl.pallas_call(
         functools.partial(gather_kernel, count),
-        out_shape=jax.ShapeDtypeStruct((count, depth, columns), w_gate.dtype),
-        in_specs=[IN_VMEM],
-        out_specs=IN_VMEM,
+        out_shape=(jax.ShapeDtypeStruct((count, depth, columns), w_gate.dtype), up, up),
+        in_specs=[IN_VMEM] * 3,
+        out_specs=(IN_VMEM,) * 3,
         scratch_shapes=[
+            VMEM((2, *up.shape), jnp.float32),
             pltpu.SemaphoreType.DMA((2, count // 2, 3)),
             pltpu.SemaphoreType.DMA((2, count // 2, 3)),
             pltpu.SemaphoreType.DMA((2, count // 2)),
@@ -144,18 +197,21 @@
             collective_id=0, has_side_effects=True, vmem_limit_bytes=40 * 2**20
         ),
         name="gather_weight",
-    )(w_gate)
+    )(w_gate, x_next, x_prev)
 
 
 def reduce_kernel(
     count,
     peers,
-    grad_ref,
+    x_ref,
+    up_ref,
+    w_ref,
     term_ref,
-    part_ref,
     total_ref,
     terms_ref,
     parts_ref,
+    grad_ref,
+    part_ref,
     side_buf,
     out_buf,
     in_buf,
@@ -178,8 +234,10 @@
 ):
     fs, rep, tp = lax.axis_index("fs"), lax.axis_index("rep"), lax.axis_index("tp")
     half = count // 2
-    quarter = grad_ref.shape[1] // 4
-    rows, other_rows = piece_rows(rep, quarter), piece_rows(1 - rep, quarter)[0]
+    depth, columns = grad_ref.shape[1:]
+    tile = column_tile(columns)
+    rows = piece_rows(rep, depth, depth // 4)
+    other_rows = piece_rows(1 - rep, depth, depth // 4)[0]
     spot = ring_spot(fs, count)
 
     def at(offset):
@@ -196,8 +254,6 @@
         remote(part_ref, parts_ref.at[tp], peer_send.at[i], peer_recv.at[i], device)
         for i, device in enumerate(others)
     ]
-    for copy in spread:
-        copy.start()
 
     def side(offset):
         slot = offset % count
@@ -211,9 +267,30 @@
         )
 
     order = [half] + [sign * k for k in range(half - 1, 0, -1) for sign in (1, -1)] + [0]
-    sides = [side(offset) for offset in order]
-    for copy in sides:
-        copy.start()
+    sides = []
+
+    def multiply(offset):
+        owner = at(offset)
+
+        @pl.loop(0, columns // tile)
+        def _(index):
+            where = pl.ds(pl.multiple_of(index * tile, 128), tile)
+            grad_ref[owner, :, where] = jnp.dot(
+                x_ref[owner], up_ref[:, where], preferred_element_type=jnp.float32
+            ).astype(grad_ref.dtype)
+
+        sides.append(side(offset))
+        sides[-1].start()
+
+    joined = max(1, 128 // depth)
+
+    def input_part(group):
+        block = w_ref[group * joined : (group + 1) * joined].reshape(joined * depth, columns)
+        product = lax.dot_general(
+            up_ref[...], block, (((1,), (1,)), ((), ())), preferred_element_type=jnp.float32
+        )
+        first = group * joined * depth
+        part_ref[:, first : first + joined * depth] = product.astype(part_ref.dtype)
 
     def parts(way, step):
         return (0, 1, 2) if step > 1 else ((0, 1), (2,))[way]
@@ -248,9 +325,15 @@
         sems = (way, step - 1)
         return remote(block, block, term_send.at[sems], term_recv.at[sems], toward[way])
 
-    for way, step, piece in ((0, 1, 1), (1, 1, 2), (0, 2, 2), (1, 2, 1)):
-        send(way, step, piece, True)
-    parts_ref[tp] = part_ref[...]
+    multiply(order[0])
+    send(0, 1, 1, True)
+    send(1, 1, 2, True)
+    multiply(order[1])
+    send(0, 2, 2, True)
+    multiply(order[2])
+    send(1, 2, 1, True)
+    for offset in order[3:]:
+        multiply(offset)
     pair.wait()
     term_buf[fs] = term_ref[...] + term_in[...]
     term_hops = [term_hop(way, 1) for way in range(2)]
@@ -269,6 +352,12 @@
             if step + 1 < half or way == 0:
                 term_hops.append(term_hop(way, step + 1))
                 term_hops[-1].start()
+        groups = count // joined
+        for group in range((step - 1) * groups // (half - 1), step * groups // (half - 1)):
+            input_part(group)
+    for copy in spread:
+        copy.start()
+    parts_ref[tp] = part_ref[...]
     lasts = {}
     side(0).wait_recv()
     for piece in (1, 2, 0):
@@ -300,8 +389,9 @@
         copy.wait()
 
 
-def reduce_gradients(grad_blocks, terms, part, peers):
-    count, depth, columns = grad_blocks.shape
+def reduce_gradients(x_blocks, grad_up, gathered, terms, peers):
+    count, depth, columns = gathered.shape
+    part = jax.ShapeDtypeStruct((grad_up.shape[0], count * depth), jnp.bfloat16)
     half, quarter = count // 2, depth // 4
     dma = pltpu.SemaphoreType.DMA
     pieces = (2, half, 3)
@@ -312,9 +402,11 @@
             jax.ShapeDtypeStruct(terms.shape, jnp.float32),
             jax.ShapeDtypeStruct((peers, *part.shape), part.dtype),
         ),
-        in_specs=[IN_VMEM] * 3,
+        in_specs=[IN_VMEM] * 4,
         out_specs=(IN_VMEM,) * 3,
         scratch_shapes=[
+            VMEM(gathered.shape, jnp.bfloat16),
+            VMEM(part.shape, part.dtype),
             VMEM((count, quarter, columns), jnp.bfloat16),
             VMEM((*pieces, quarter, columns), jnp.bfloat16),
             VMEM((*pieces, quarter, columns), jnp.bfloat16),
@@ -339,7 +431,7 @@
             collective_id=1, has_side_effects=True, vmem_limit_bytes=56 * 2**20
         ),
         name="reduce_gradients",
-    )(grad_blocks, terms, part)
+    )(x_blocks, grad_up, gathered, terms)
 
 
 def per_device(
@@ -359,11 +451,7 @@
     tap_count = conv_taps.shape[0]
     position = jnp.arange(row_count) % SEQ_LEN
     fs_count = lax.axis_size("fs")
-    gathered = gather_weight(w_gate, fs_count).reshape(fs_count * w_gate.shape[0], w_gate.shape[1])
-    up_next = jnp.dot(x_next, gathered, preferred_element_type=jnp.float32)
-    up_prev = jnp.dot(x_prev, gathered, preferred_element_type=jnp.float32)
-    up_next = up_next.astype(jnp.bfloat16)
-    up_prev = up_prev.astype(jnp.bfloat16)
+    gathered, up_next, up_prev = gather_weight(w_gate, x_next, x_prev, fs_count)
     gate_next = convolve(up_next, conv_taps, conv_bias, position)
     hidden_next = (gate_next * jax.nn.sigmoid(gate_next) * value_next.astype(jnp.float32)).astype(
         jnp.bfloat16
@@ -384,10 +472,6 @@
             grad_gate, tap_count - 1 - tap_index, position
         )
     grad_up = grad_up.astype(jnp.bfloat16)
-    contract_units = (((1,), (1,)), ((), ()))
-    partial_input = lax.dot_general(
-        grad_up, gathered, contract_units, preferred_element_type=jnp.float32
-    )
     rep_count = lax.axis_size("rep")
     grad_scale = float(row_count * rep_count * fs_count) ** (-0.5)
     up_values = up_prev.astype(jnp.float32)
@@ -399,15 +483,13 @@
         + [jnp.sum(grad_gate, axis=0)],
         axis=0,
     )
-    grad_blocks = (
-        lax.dot_general(x_prev, grad_up, (((0,), (0,)), ((), ())), preferred_element_type=jnp.float32)
-        .astype(jnp.bfloat16)
-        .reshape(fs_count, *w_gate.shape)
-    )
-    grad_rows, terms, partials = reduce_gradients(
-        grad_blocks, terms, partial_input.astype(jnp.bfloat16), lax.axis_size("tp")
-    )
-    grad_input = jnp.sum(partials.astype(jnp.float32), axis=0).astype(jnp.bfloat16)
+    peers = lax.axis_size("tp")
+    x_blocks = x_prev.T.reshape(fs_count, w_gate.shape[0], row_count)
+    grad_rows, terms, partials = reduce_gradients(x_blocks, grad_up, gathered, terms, peers)
+    grad_input = partials[0].astype(jnp.float32)
+    for peer in range(1, peers):
+        grad_input = grad_input + partials[peer].astype(jnp.float32)
+    grad_input = grad_input.astype(jnp.bfloat16)
     return (
         hidden_next,
         grad_input,

time: 163 us -> 149 us (0.914)
  matrix products: 14.3 us -> 0 us
    dot_general x4 -> x0, matrix products: 14.3 us -> none  [the longest x1 5.35 us: per_device(): lax.dot_general(x_prev, grad_up, (((0,), (0,)), ((), ())), preferred_elem...]
    convert_element_type x1 -> x0, local copies, waits for them, and re-layouts: 8.67 us -> none  [per_device(): grad_blocks = lax.dot_general(x_prev, grad_up, (((0,), (0,)), ((), ())),...]
    unnamed x22 -> x30, local copies, waits for them, and re-layouts: 1.19 us -> 7.89 us
    reduce_sum x1 -> x0, other arithmetic: 4.33 us -> none  [per_device(): jnp.sum(partials.astype(jnp.float32), axis=0).astype(jnp.bfloat16)]
    convert_element_type x0 -> x1, other arithmetic: none -> 3.85 us  [per_device(): grad_input = grad_input.astype(jnp.bfloat16)]
where the time goes in v2:
time: 149 us; the launch traced here: 148 us
  Pallas kernels  118 us (79%)
  other arithmetic  18 us (12%)
  local copies, waits for them, and re-layouts  11.1 us (7%)
    pallas_call x1, Pallas kernels, reduce_gradients(): pl.pallas_call(functools.partial(reduce_kernel, count, peers), out_shape=...  64.7 us
    pallas_call x1, Pallas kernels, gather_weight(): pl.pallas_call(functools.partial(gather_kernel, count), out_shape=(jax.Sh...  53.5 us
    unnamed x30, local copies, waits for them, and re-layouts  7.89 us
    convert_element_type x1, other arithmetic, per_device(): grad_value = (cot_values * gate_prev * sigmoid_gate).astype(jnp.bfloat16)  5.74 us
    convert_element_type x1, other arithmetic, per_device(): grad_input = grad_input.astype(jnp.bfloat16)  3.85 us
    reduce_sum x1, other arithmetic, per_device(): jnp.sum(grad_gate * lagged(up_values, tap_count - 1 - tap_index, position...  3.13 us

profile of v2, /device:TPU:0, one launch (start us, length us, event | category | flops | bytes accessed | tf_op | source)
XLA Modules:
  0.0 148.3 jit_solution(14521452653764022676)
XLA Ops:
  0.6 1.4 copy-done.1
  2.0 1.4 copy-done.3
  3.5 1.1 copy-done.4
  4.6 53.5 %gather_weight.1 = (bf16[8,256,1536]{2,1,0:T(8,128)(2,1)S(1)}, bf16[384,1536]{1,0:T(8,128)(2,1)S(1)}, bf16[384,1536]{1,0:T(8,128)(2,1)S(1)}) custom-call(bf16[256,1536]{1,0:T(8,128)(2,1)S(1)} %copy-done.4, bf16[384,2048]{1,0:T(8,128)(2,1)S(1)} %copy-done.3, bf16[384,2048]{1,0:T(8,128)(2,1)S(1)} %copy-done.1), custom_call_target="tpu_custom_call" | custom-call | tf_op jit(solution)/shard_map/gather_weight/pallas_call | solution.py:184
  58.1 2.7 %copy-done = bf16[8,256,1536]{2,1,0:T(8,128)(2,1)} copy-done((bf16[8,256,1536]{2,1,0:T(8,128)(2,1)}, bf16[8,256,1536]{2,1,0:T(8,128)(2,1)S(1)}, u32[]{:S(2)}) %copy-start) | copy-done | bytes 6291480
  60.8 0.3 slice.62
  61.1 0.3 slice.63
  61.4 0.3 slice.60
  61.7 0.3 slice.61
  62.0 0.4 copy-done.12
  62.5 0.5 copy-done.5
  63.0 0.4 copy-done.8
  63.3 5.7 %fusion.3 = (bf16[384,1536]{1,0:T(8,128)(2,1)}, f32[384,1536]{1,0:T(8,128)S(1)}, bf16[384,1536]{1,0:T(8,128)(2,1)}) fusion(bf16[384,1536]{1,0:T(8,128)(2,1)S(1)} %copy-done.5, bf16[384,1536]{1,0:T(8,128)(2,1)S(1)} %get-tuple-element.13, pred[384]{0:T(512)(128)(4,1)S(1)} %get-tuple-element.29, f32[1536]{0:T(1024)S(1)} %get-tuple-element.23, ...), kind=kLoop, calls=%fused_computation.6 | loop fusion | flops 20054016 | bytes 18863232 | tf_op jit(solution)/shard_map/convert_element_type | solution.py:462
  69.1 3.1 %multiply_reduce_fusion.2 = (f32[1536]{0:T(1024)S(1)}, f32[1536]{0:T(1024)S(1)}, f32[1536]{0:T(1024)S(1)}, f32[1536]{0:T(1024)S(1)}, f32[384,1536]{1,0:T(8,128)S(1)}) fusion(f32[382,1536]{1,0:T(8,128)S(1)} %slice.62, pred[384]{0:T(512)(128)(4,1)S(1)} %fusion.12, bf16[384,1536]{1,0:T(8,128)(2,1)S(1)} %get-tuple-element.13, ...), kind=kLoop, calls=%fused_computation.9 | loop fusion | flops 12969984 | bytes 12983424 | tf_op jit(solution)/shard_map/reduce_sum | solution.py:480
  72.3 0.6 pad_maximum_fusion.term_ref
  72.9 0.2 slice.64
  73.2 0.2 slice.65
  73.4 2.0 %add_convert_fusion.1.up_ref = bf16[384,1536]{1,0:T(8,128)(2,1)} fusion(f32[384,1536]{1,0:T(8,128)S(1)} %get-tuple-element.27, f32[383,1536]{1,0:T(8,128)S(1)} %slice.65, f32[382,1536]{1,0:T(8,128)S(1)} %slice.64, f32[1536]{0:T(1024)S(1)} %get-tuple-element.23, f32[1536]{0:T(1024)S(1)} %get-tuple-element.24, f32[1536]{0:T(1024)S(1)} %get-tuple-element.22, ...), kind=kLoop, calls=%fused_computation.10 | loop fusion | flops 5308416 | bytes 8258688 | tf_op jit(solution)/shard_map/convert_element_type | solution.py:474
  75.4 1.6 %copy.17 = bf16[2048,384]{1,0:T(8,128)(2,1)} copy(bf16[2048,384]{0,1:T(8,128)(2,1)S(1)} %bitcast.4) | data formatting | bytes 3145728 | tf_op jit(solution)/shard_map/transpose | solution.py:487
  77.0 64.7 %reduce_gradients.1 = (f32[256,1536]{1,0:T(8,128)}, f32[4,1536]{1,0:T(4,128)}, bf16[2,384,2048]{2,1,0:T(8,128)(2,1)}) custom-call(bf16[8,256,384]{2,1,0:T(8,128)(2,1)} %bitcast.5, bf16[384,1536]{1,0:T(8,128)(2,1)} %add_convert_fusion.1.up_ref, bf16[8,256,1536]{2,1,0:T(8,128)(2,1)} %copy-done, f32[4,1536]{1,0:T(4,128)} %pad_maximum_fusion.term_ref), custom_call_target="tpu_custom_call" | custom-call | tf_op jit(solution)/shard_map/reduce_gradients/pallas_call | solution.py:398
  141.8 3.8 %fusion.4 = bf16[384,2048]{1,0:T(8,128)(2,1)} fusion(bf16[2,384,2048]{2,1,0:T(8,128)(2,1)} %get-tuple-element.15), kind=kLoop, calls=%fused_computation.16 | loop fusion | flops 3145728 | bytes 4718592 | tf_op jit(solution)/shard_map/convert_element_type | solution.py:492
  145.7 1.4 multiply_add_fusion.1
  147.0 0.6 multiply_add_fusion.2
  147.7 0.6 add.123
  (33 shorter events, 0.2 us)
Async XLA Ops:
  0.6 1.4 copy-start.1
  2.0 1.4 copy-start.3
  3.5 1.1 copy-start.4
  58.1 2.7 %copy-start = (bf16[8,256,1536]{2,1,0:T(8,128)(2,1)}, bf16[8,256,1536]{2,1,0:T(8,128)(2,1)S(1)}, u32[]{:S(2)}) copy-start(bf16[8,256,1536]{2,1,0:T(8,128)(2,1)S(1)} %get-tuple-element.14.w_ref) | copy-start | bytes 18874372
  61.7 0.7 copy-start.12
  61.7 1.3 copy-start.5
  61.7 1.6 %copy-start.8 = (bf16[384,1536]{1,0:T(8,128)(2,1)S(1)}, bf16[384,1536]{1,0:T(8,128)(2,1)}, u32[]{:S(2)}) copy-start(bf16[384,1536]{1,0:T(8,128)(2,1)} %param.12) | copy-start | bytes 3538948
  61.7 1.6 %copy-start.13 = (f32[1536]{0:T(1024)S(1)}, f32[1536]{0:T(1024)}, u32[]{:S(2)}) copy-start(f32[1536]{0:T(1024)} %param.18) | copy-start | bytes 18436
  63.3 5.7 %copy-start.9 = (bf16[384,1536]{1,0:T(8,128)(2,1)S(1)}, bf16[384,1536]{1,0:T(8,128)(2,1)}, u32[]{:S(2)}) copy-start(bf16[384,1536]{1,0:T(8,128)(2,1)} %param.14) | copy-start | bytes 3538948
  73.4 2.0 %copy-start.2 = (bf16[384,2048]{1,0:T(8,128)(2,1)S(1)}, bf16[384,2048]{1,0:T(8,128)(2,1)}, u32[]{:S(2)}) copy-start(bf16[384,2048]{1,0:T(8,128)(2,1)} %x_prev_ref.1) | copy-start | bytes 4718596
  141.7 3.9 %copy-start.6 = (f32[256,1536]{1,0:T(8,128)S(1)}, f32[256,1536]{1,0:T(8,128)}, u32[]{:S(2)}) copy-start(f32[256,1536]{1,0:T(8,128)} %param.19) | copy-start | bytes 4718596
  141.8 3.9 %copy-start.7 = (f32[256,1536]{1,0:T(8,128)S(1)}, f32[256,1536]{1,0:T(8,128)}, u32[]{:S(2)}) copy-start(f32[256,1536]{1,0:T(8,128)} %get-tuple-element.16) | copy-start | bytes 4718596
  145.6 1.4 copy-start.10
  145.6 1.4 copy-start.11
  145.6 2.0 %copy-start.14 = (f32[1536]{0:T(1024)S(1)}, f32[1536]{0:T(1024)}, u32[]{:S(2)}) copy-start(f32[1536]{0:T(1024)} %param.21) | copy-start | bytes 18436

commit v3 on v2

--- a/solution.py
+++ b/solution.py
@@ -13,32 +13,91 @@
 IN_VMEM = pl.BlockSpec(memory_space=pltpu.VMEM)
 
 
-def lagged(values, offset, position):
-    count_rows = values.shape[0]
-    shifted_rows = jnp.concatenate(
-        (jnp.zeros((offset, values.shape[1]), values.dtype), values[: count_rows - offset]), axis=0
-    )
-    return jnp.where((position >= offset)[:, None], shifted_rows, jnp.zeros_like(shifted_rows))
-
-
-def leading(values, offset, position):
-    shifted_rows = jnp.concatenate(
-        (values[offset:], jnp.zeros((offset, values.shape[1]), values.dtype)), axis=0
-    )
-    return jnp.where(
-        (position < SEQ_LEN - offset)[:, None], shifted_rows, jnp.zeros_like(shifted_rows)
-    )
-
-
-def convolve(up_rows, conv_taps, conv_bias, position):
-    values = up_rows.astype(jnp.float32)
+def gates_kernel(
+    up_next_ref,
+    value_next_ref,
+    up_prev_ref,
+    value_prev_ref,
+    cotangent_ref,
+    taps_ref,
+    bias_ref,
+    hidden_ref,
+    grad_value_ref,
+    grad_up_ref,
+    terms_ref,
+):
+    tap_count = taps_ref.shape[0]
+    row_count, tile = up_next_ref.shape
+    position = lax.broadcasted_iota(jnp.int32, (SEQ_LEN, tile), 0)
+    lags = [tap_count - 1 - tap for tap in range(tap_count)]
+    taps = [taps_ref[tap : tap + 1, :] for tap in range(tap_count)]
+    bias = bias_ref[...]
+
+    def lagged(values, offset):
+        if offset == 0:
+            return values
+        return jnp.where(position >= offset, pltpu.roll(values, offset, 0), 0.0)
+
+    def leading(values, offset):
+        if offset == 0:
+            return values
+        shifted = pltpu.roll(values, SEQ_LEN - offset, 0)
+        return jnp.where(position < SEQ_LEN - offset, shifted, 0.0)
+
+    def mixed(pieces, start):
+        for tap, piece in zip(taps, pieces):
+            start = start + tap * piece
+        return start
+
+    sums = [jnp.zeros((1, tile), jnp.float32) for _ in range(tap_count + 1)]
+    for first in range(0, row_count, SEQ_LEN):
+        rows = slice(first, first + SEQ_LEN)
+        up = up_next_ref[rows, :].astype(jnp.float32)
+        gate = mixed([lagged(up, lag) for lag in lags], bias)
+        hidden = gate * jax.nn.sigmoid(gate) * value_next_ref[rows, :].astype(jnp.float32)
+        hidden_ref[rows, :] = hidden.astype(hidden_ref.dtype)
+        up = up_prev_ref[rows, :].astype(jnp.float32)
+        lagged_up = [lagged(up, lag) for lag in lags]
+        gate = mixed(lagged_up, bias)
+        sigmoid = jax.nn.sigmoid(gate)
+        cot = cotangent_ref[rows, :].astype(jnp.float32)
+        grad_value_ref[rows, :] = (cot * gate * sigmoid).astype(grad_value_ref.dtype)
+        value = value_prev_ref[rows, :].astype(jnp.float32)
+        grad_gate = cot * value * sigmoid * (1.0 + gate * (1.0 - sigmoid))
+        grad_up = mixed([leading(grad_gate, lag) for lag in lags], 0.0)
+        grad_up_ref[rows, :] = grad_up.astype(grad_up_ref.dtype)
+        products = [grad_gate * piece for piece in lagged_up] + [grad_gate]
+        sums = [
+            total + jnp.sum(product, axis=0, keepdims=True)
+            for total, product in zip(sums, products)
+        ]
+    for index, total in enumerate(sums):
+        terms_ref[index : index + 1, :] = total
+
+
+def gates(up_next, value_next, up_prev, value_prev, cotangent, conv_taps, conv_bias):
+    row_count, columns = up_next.shape
     tap_count = conv_taps.shape[0]
-    result = jnp.zeros(values.shape, jnp.float32) + conv_bias[None, :]
-    for tap_index in range(tap_count):
-        result = result + conv_taps[tap_index][None, :] * lagged(
-            values, tap_count - 1 - tap_index, position
-        )
-    return result
+    tile = 256 if columns % 256 == 0 else 128
+    tall = pl.BlockSpec((row_count, tile), lambda index: (0, index))
+
+    def flat(height):
+        return pl.BlockSpec((height, tile), lambda index: (0, index))
+
+    large = jax.ShapeDtypeStruct((row_count, columns), jnp.bfloat16)
+    return pl.pallas_call(
+        gates_kernel,
+        grid=(columns // tile,),
+        out_shape=(
+            large,
+            large,
+            large,
+            jax.ShapeDtypeStruct((tap_count + 1, columns), jnp.float32),
+        ),
+        in_specs=[tall] * 5 + [flat(tap_count), flat(1)],
+        out_specs=(tall, tall, tall, flat(tap_count + 1)),
+        name="gates",
+    )(up_next, value_next, up_prev, value_prev, cotangent, conv_taps, conv_bias[None, :])
 
 
 def ring_spot(index, count):
@@ -449,40 +508,13 @@
 ):
     row_count = x_next.shape[0]
     tap_count = conv_taps.shape[0]
-    position = jnp.arange(row_count) % SEQ_LEN
     fs_count = lax.axis_size("fs")
     gathered, up_next, up_prev = gather_weight(w_gate, x_next, x_prev, fs_count)
-    gate_next = convolve(up_next, conv_taps, conv_bias, position)
-    hidden_next = (gate_next * jax.nn.sigmoid(gate_next) * value_next.astype(jnp.float32)).astype(
-        jnp.bfloat16
+    hidden_next, grad_value, grad_up, terms = gates(
+        up_next, value_next, up_prev, value_prev, cotangent, conv_taps, conv_bias
     )
-    gate_prev = convolve(up_prev, conv_taps, conv_bias, position)
-    sigmoid_gate = jax.nn.sigmoid(gate_prev)
-    cot_values = cotangent.astype(jnp.float32)
-    grad_value = (cot_values * gate_prev * sigmoid_gate).astype(jnp.bfloat16)
-    grad_gate = (
-        cot_values
-        * value_prev.astype(jnp.float32)
-        * sigmoid_gate
-        * (1.0 + gate_prev * (1.0 - sigmoid_gate))
-    )
-    grad_up = jnp.zeros(grad_gate.shape, jnp.float32)
-    for tap_index in range(tap_count):
-        grad_up = grad_up + conv_taps[tap_index][None, :] * leading(
-            grad_gate, tap_count - 1 - tap_index, position
-        )
-    grad_up = grad_up.astype(jnp.bfloat16)
     rep_count = lax.axis_size("rep")
     grad_scale = float(row_count * rep_count * fs_count) ** (-0.5)
-    up_values = up_prev.astype(jnp.float32)
-    terms = jnp.stack(
-        [
-            jnp.sum(grad_gate * lagged(up_values, tap_count - 1 - tap_index, position), axis=0)
-            for tap_index in range(tap_count)
-        ]
-        + [jnp.sum(grad_gate, axis=0)],
-        axis=0,
-    )
     peers = lax.axis_size("tp")
     x_blocks = x_prev.T.reshape(fs_count, w_gate.shape[0], row_count)
     grad_rows, terms, partials = reduce_gradients(x_blocks, grad_up, gathered, terms, peers)

time: 149 us -> 144 us (0.966)
  other arithmetic: 18 us -> 6.47 us
  Pallas kernels: 118 us -> 126 us
    pallas_call x0 -> x1, Pallas kernels: none -> 8.02 us  [gates(): pl.pallas_call(gates_kernel, grid=(columns // tile,), out_shape=(large, l...]
    convert_element_type x2 -> x0, other arithmetic: 7.73 us -> none  [the longest x1 5.74 us: per_device(): grad_value = (cot_values * gate_prev * sigmoid_gate).astype(jnp.bfloat16)]
    reduce_sum x1 -> x0, other arithmetic: 3.13 us -> none  [per_device(): jnp.sum(grad_gate * lagged(up_values, tap_count - 1 - tap_index, position...]
    unnamed x30 -> x22, local copies, waits for them, and re-layouts: 7.89 us -> 5.86 us
    slice x7 -> x0, local copies, waits for them, and re-layouts: 1.66 us -> none  [the longest x4 1.11 us: lagged(): values[:count_rows - offset]]
where the time goes in v3:
time: 144 us; the launch traced here: 143 us
  Pallas kernels  126 us (88%)
  local copies, waits for them, and re-layouts  9.88 us (7%)
  other arithmetic  6.47 us (4%)
    pallas_call x1, Pallas kernels, reduce_gradients(): pl.pallas_call(functools.partial(reduce_kernel, count, peers), out_shape=...  64.8 us
    pallas_call x1, Pallas kernels, gather_weight(): pl.pallas_call(functools.partial(gather_kernel, count), out_shape=(jax.Sh...  53.5 us
    pallas_call x1, Pallas kernels, gates(): pl.pallas_call(gates_kernel, grid=(columns // tile,), out_shape=(large, l...  8.02 us
    unnamed x22, local copies, waits for them, and re-layouts  5.86 us
    convert_element_type x1, other arithmetic, per_device(): grad_input = grad_input.astype(jnp.bfloat16)  3.85 us

profile of v3, /device:TPU:0, one launch (start us, length us, event | category | flops | bytes accessed | tf_op | source)
XLA Modules:
  0.0 143.4 jit_solution(8665806706847685107)
XLA Ops:
  0.6 1.3 broadcast_in_dim.3.bias_ref
  1.9 2.7 %copy.17 = bf16[2048,384]{1,0:T(8,128)(2,1)} copy(bf16[2048,384]{0,1:T(8,128)(2,1)} %bitcast.4) | data formatting | bytes 3145728 | tf_op jit(solution)/shard_map/transpose | solution.py:519
  4.7 0.0 copy-done.1
  4.7 0.0 copy-done.2
  4.7 1.1 copy-done.5
  5.8 53.5 %gather_weight.1 = (bf16[8,256,1536]{2,1,0:T(8,128)(2,1)S(1)}, bf16[384,1536]{1,0:T(8,128)(2,1)S(1)}, bf16[384,1536]{1,0:T(8,128)(2,1)S(1)}) custom-call(bf16[256,1536]{1,0:T(8,128)(2,1)S(1)} %copy-done.5, bf16[384,2048]{1,0:T(8,128)(2,1)S(1)} %copy-done.2, bf16[384,2048]{1,0:T(8,128)(2,1)S(1)} %copy-done.1), custom_call_target="tpu_custom_call" | custom-call | tf_op jit(solution)/shard_map/gather_weight/pallas_call | solution.py:243
  59.4 0.0 copy-start
  59.4 2.6 %copy-done = bf16[8,256,1536]{2,1,0:T(8,128)(2,1)} copy-done((bf16[8,256,1536]{2,1,0:T(8,128)(2,1)}, bf16[8,256,1536]{2,1,0:T(8,128)(2,1)S(1)}, u32[]{:S(2)}) %copy-start) | copy-done | bytes 6291480
  62.0 1.0 copy-done.3
  63.0 1.0 copy-done.4
  64.1 8.0 %gates.1 = (bf16[384,1536]{1,0:T(8,128)(2,1)}, bf16[384,1536]{1,0:T(8,128)(2,1)}, bf16[384,1536]{1,0:T(8,128)(2,1)}, f32[4,1536]{1,0:T(4,128)}) custom-call(bf16[384,1536]{1,0:T(8,128)(2,1)} %copy-done.3, bf16[384,1536]{1,0:T(8,128)(2,1)} %value_next_ref.1, bf16[384,1536]{1,0:T(8,128)(2,1)} %copy-done.4, bf16[384,1536]{1,0:T(8,128)(2,1)} %value_prev_ref.1, ...), custom_call_target="tpu_custom_call" | custom-call | tf_op jit(solution)/shard_map/gates/pallas_call | solution.py:88
  72.1 64.8 %reduce_gradients.1 = (f32[256,1536]{1,0:T(8,128)}, f32[4,1536]{1,0:T(4,128)}, bf16[2,384,2048]{2,1,0:T(8,128)(2,1)}) custom-call(bf16[8,256,384]{2,1,0:T(8,128)(2,1)} %bitcast.5, bf16[384,1536]{1,0:T(8,128)(2,1)} %get-tuple-element.19.up_ref, bf16[8,256,1536]{2,1,0:T(8,128)(2,1)} %copy-done, f32[4,1536]{1,0:T(4,128)} %get-tuple-element.21.term_ref), custom_call_target="tpu_custom_call" | custom-call | tf_op jit(solution)/shard_map/reduce_gradients/pallas_call | solution.py:457
  136.9 0.0 copy-start.8
  136.9 0.0 copy-start.9
  136.9 0.0 copy-start.10
  136.9 0.0 copy-start.6
  136.9 0.0 copy-start.7
  136.9 3.8 %fusion = bf16[384,2048]{1,0:T(8,128)(2,1)} fusion(bf16[2,384,2048]{2,1,0:T(8,128)(2,1)} %get-tuple-element.22), kind=kLoop, calls=%fused_computation.1 | loop fusion | flops 3145728 | bytes 4718592 | tf_op jit(solution)/shard_map/convert_element_type | solution.py:524
  140.8 0.0 copy-done.8
  140.8 0.0 copy-done.9
  140.8 0.6 multiply_add_fusion.1
  141.4 0.0 copy-done.10
  141.4 0.6 add.16
  142.0 1.4 multiply_add_fusion
  (8 shorter events, 0.0 us)
Async XLA Ops:
  1.9 2.7 %copy-start.1 = (bf16[384,2048]{1,0:T(8,128)(2,1)S(1)}, bf16[384,2048]{1,0:T(8,128)(2,1)}, u32[]{:S(2)}) copy-start(bf16[384,2048]{1,0:T(8,128)(2,1)} %x_prev_ref.1) | copy-start | bytes 4718596
  1.9 2.7 %copy-start.2 = (bf16[384,2048]{1,0:T(8,128)(2,1)S(1)}, bf16[384,2048]{1,0:T(8,128)(2,1)}, u32[]{:S(2)}) copy-start(bf16[384,2048]{1,0:T(8,128)(2,1)} %x_next_ref.1) | copy-start | bytes 4718596
  4.7 1.1 copy-start.5
  59.4 2.7 %copy-start = (bf16[8,256,1536]{2,1,0:T(8,128)(2,1)}, bf16[8,256,1536]{2,1,0:T(8,128)(2,1)S(1)}, u32[]{:S(2)}) copy-start(bf16[8,256,1536]{2,1,0:T(8,128)(2,1)S(1)} %get-tuple-element.20.w_ref) | copy-start | bytes 18874372
  62.0 1.0 copy-start.3
  63.0 1.0 copy-start.4
  136.9 3.9 %copy-start.8 = (f32[4,1536]{1,0:T(4,128)S(1)}, f32[4,1536]{1,0:T(4,128)}, u32[]{:S(2)}) copy-start(f32[4,1536]{1,0:T(4,128)} %get-tuple-element.25) | copy-start | bytes 73732
  136.9 3.9 %copy-start.9 = (f32[3,1536]{1,0:T(4,128)S(1)}, f32[3,1536]{1,0:T(4,128)}, u32[]{:S(2)}) copy-start(f32[3,1536]{1,0:T(4,128)} %param.20) | copy-start | bytes 55300
  136.9 4.5 %copy-start.10 = (f32[1536]{0:T(1024)S(1)}, f32[1536]{0:T(1024)}, u32[]{:S(2)}) copy-start(f32[1536]{0:T(1024)} %param.21) | copy-start | bytes 18436
  136.9 5.1 %copy-start.6 = (f32[256,1536]{1,0:T(8,128)S(1)}, f32[256,1536]{1,0:T(8,128)}, u32[]{:S(2)}) copy-start(f32[256,1536]{1,0:T(8,128)} %param.19) | copy-start | bytes 4718596
  136.9 5.1 %copy-start.7 = (f32[256,1536]{1,0:T(8,128)S(1)}, f32[256,1536]{1,0:T(8,128)}, u32[]{:S(2)}) copy-start(f32[256,1536]{1,0:T(8,128)} %get-tuple-element.24) | copy-start | bytes 4718596
